TPU v7x, 32 devices: a whole 2x2x4 slice. The times are simulated.
32 devices in a mesh: grp: 2 (over y), ep: 16 (over z, x, core), tp: 1.
Axes of the slice: x: 2, y: 2, z: 4, core: 2. Of those that a mesh axis runs over, the one named last changes fastest.
Arguments:
- tokens: bfloat16 [2048, 2048], P(('grp', 'ep')), parts along dimension 0, may hold values from -6 to 6
- norm_gain: float32 [2048], replicated, may hold values from 0.1 to 1.9
- routes: int32 [2048, 6], P(('grp', 'ep')), parts along dimension 0, may hold values from 0 to 15, all different within a row; in each aligned block of 64 rows (0 to 63, 64 to 127, ...) at most 48 rows name the same one
- route_weights: float32 [2048, 6], P(('grp', 'ep')), parts along dimension 0, may hold values from 0.05 to 1
- w_gate: bfloat16 [16, 2048, 2048], P('ep', None, 'tp'), may hold values from -0.125 to 0.125
- w_up: bfloat16 [16, 2048, 2048], P('ep', None, 'tp'), may hold values from -0.125 to 0.125
- w_down: bfloat16 [16, 2048, 2048], P('ep', 'tp'), may hold values from -4 to 4
- final_gain: float32 [2048], P('tp'), may hold values from 0.1 to 1.9
Outputs:
- mixed_out: bfloat16 [2048, 2048], P(('grp', 'ep'), 'tp'), parts along dimension 0
There are 2 independent parts, one for each index of `grp`. A program takes and returns all parts, laid end to end along the dimension named above; an argument that names none is the same for every part. Nothing has to cross between parts.
Inputs may be any that keep to these rules, and one draw needn't show every extreme that they name: `routes`: each row names 6 different experts; within the rows of one index of ep no expert is named by more than 48 rows, and in every draw some expert is named by exactly 48 rows of some index.
All inputs are finite; a program needn't handle non-finite values.
Results may differ from a plain program's by a relative error of at most 0.015.
Values may be sent and summed in bfloat16 or wider, within the bound.
No kernel may reach another device: no remote copies, remote signals or barrier semaphores. Data moves between devices by JAX's collectives and lax.ppermute only.
A program may use at most 64 MiB of HBM per device.

v0:
```python
import jax
import jax.numpy as jnp
from jax import lax
from jax.sharding import PartitionSpec as P

TOP_K = 6
EPS = 1e-06


def slot_table(route_rows, experts_all, capacity):
    flattened = route_rows.reshape(-1)
    matches = (flattened[:, None] == jnp.arange(experts_all, dtype=jnp.int32)[None, :]).astype(
        jnp.int32
    )
    earlier = jnp.cumsum(matches, axis=0) - matches
    slot_of = jnp.sum(earlier * matches, axis=1)
    return (flattened * capacity + slot_of).reshape(route_rows.shape)


def per_device(tokens, norm_gain, routes, route_weights, w_gate, w_up, w_down, final_gain):
    tok_count, features = tokens.shape
    ep_size = lax.axis_size("ep")
    exp_local = w_gate.shape[0]
    experts_all = exp_local * ep_size
    capacity = max(2, min(tok_count, 2 * tok_count * TOP_K // experts_all))
    slot_count = experts_all * capacity
    tokens_f = tokens.astype(jnp.float32)
    inverse = lax.rsqrt(jnp.mean(tokens_f * tokens_f, axis=1, keepdims=True) + EPS)
    normed = (tokens_f * inverse * norm_gain[None, :]).astype(jnp.bfloat16)
    places = slot_table(routes, experts_all, capacity)
    slot_ids = jnp.arange(slot_count, dtype=jnp.int32)
    matched = places[:, :, None] == slot_ids[None, None, :]
    selector = jnp.sum(matched.astype(jnp.float32), axis=1).T.astype(jnp.bfloat16)
    combine_rows = jnp.sum(jnp.where(matched, route_weights[:, :, None], 0.0), axis=1)
    outgoing = jnp.dot(selector, normed, preferred_element_type=jnp.float32).astype(jnp.bfloat16)
    outgoing = outgoing.reshape(ep_size, exp_local, capacity, features)
    received = lax.all_to_all(outgoing, "ep", split_axis=0, concat_axis=0, tiled=True)
    gate_value = jnp.einsum("secd,edf->secf", received, w_gate, preferred_element_type=jnp.float32)
    up_value = jnp.einsum("secd,edf->secf", received, w_up, preferred_element_type=jnp.float32)
    hidden = (jax.nn.silu(gate_value) * up_value).astype(jnp.bfloat16)
    partial_value = jnp.einsum("secf,efd->secd", hidden, w_down, preferred_element_type=jnp.float32)
    summed = lax.psum_scatter(
        partial_value.astype(jnp.bfloat16), "tp", scatter_dimension=3, tiled=True
    )
    returned = lax.all_to_all(summed, "ep", split_axis=0, concat_axis=0, tiled=True)
    results = returned.reshape(slot_count, returned.shape[3]).astype(jnp.float32)
    combined = jnp.dot(combine_rows, results, precision=lax.Precision.HIGHEST)
    local_squares = jnp.sum(combined * combined, axis=1)
    squares_all = lax.psum(local_squares, "tp")
    inverse_out = lax.rsqrt(squares_all / features + EPS)
    return (combined * inverse_out[:, None] * final_gain[None, :]).astype(jnp.bfloat16)


def solution(mesh):
    placed = (
        P(("grp", "ep"), None),
        P(),
        P(("grp", "ep"), None),
        P(("grp", "ep"), None),
        P("ep", None, "tp"),
        P("ep", None, "tp"),
        P("ep", "tp", None),
        P("tp"),
    )
    return jax.shard_map(
        per_device, mesh=mesh, in_specs=placed, out_specs=P(("grp", "ep"), "tp"), check_vma=False
    )
```

profile of v0, /device:TPU:1, one launch (start us, length us, event | category | flops | bytes accessed | tf_op | source)
XLA Modules:
  0.0 194.4 jit_solution(3700836418852448338)
XLA Ops:
  0.0 0.8 copy.33
  0.8 0.1 eq.42
  0.9 0.1 eq.38
  1.1 1.1 fusion.33
  2.2 0.9 reduce-window.6
  3.1 0.2 slice_reduce_fusion
  3.3 0.1 fusion.42
  3.4 0.1 reduce_sum.48
  3.6 0.1 copy.36
  3.6 0.0 copy-start.1
  3.6 0.9 multiply_add_fusion
  4.5 1.1 convert_reduce_fusion
  5.6 2.4 %convolution_convert_fusion = bf16[768,2048]{1,0:T(8,128)(2,1)S(1)} fusion(bf16[64,2048]{1,0:T(8,128)(2,1)} %param.8, f32[2048]{0:T(1024)} %param.9, f32[64]{0:T(128)S(1)} %add_rsqrt_fusion.1, bf16[64,768]{1,0:T(8,128)(2,1)S(1)} %get-tuple-element.5), kind=kOutput, calls=%fused_computation.14 | convolution fusion | flops 203423744 | bytes 3514624 | tf_op jit(solution)/shard_map/dot_general | solution.py:35
  8.0 77.3 %all_to_all.10 = bf16[16,1,48,2048]{3,2,1,0:T(8,128)(2,1)S(1)} all-to-all(bf16[16,1,48,2048]{3,2,1,0:T(8,128)(2,1)S(1)} %bitcast.110), channel_id=1, replica_groups=mesh['grp'=2,'ep'=16,'tp'=1] {'ep'}, dimensions={0} | all-to-all | bytes 6291456 | tf_op jit(solution)/shard_map/all_to_all | solution.py:37
  85.3 0.0 copy-done.1
  85.3 8.6 %fusion.4 = f32[16,48,2048]{2,1,0:T(8,128)} fusion(bf16[1,2048,2048]{2,1,0:T(8,128)(2,1)S(1)} %copy-done.1, bf16[16,1,48,2048]{3,2,1,0:T(8,128)(2,1)S(1)} %all_to_all.10), kind=kOutput, calls=%fused_computation.4 | convolution fusion | flops 6442450944 | bytes 17825792 | tf_op jit(solution)/shard_map/secd,edf->secf/dot_general | solution.py:38
  93.8 22.9 %fusion.24 = bf16[16,1,48,2048]{3,2,1,0:T(8,128)(2,1)} fusion(bf16[1,2048,2048]{2,1,0:T(8,128)(2,1)} %param.14, bf16[1,2048,2048]{2,1,0:T(8,128)(2,1)} %param.13, f32[16,48,2048]{2,1,0:T(8,128)} %fusion.4, bf16[16,1,48,2048]{3,2,1,0:T(8,128)(2,1)S(1)} %all_to_all.10), kind=kOutput, calls=%fused_computation.19 | convolution fusion | flops 12895911936 | bytes 29360128 | tf_op jit(solution)/shard_map/secf,efd->secd/dot_general | solution.py:41
  116.7 0.0 copy-start
  116.7 75.0 %all_to_all.11 = bf16[16,1,48,2048]{3,2,1,0:T(8,128)(2,1)S(1)} all-to-all(bf16[16,1,48,2048]{3,2,1,0:T(8,128)(2,1)} %fusion.24), channel_id=1, replica_groups=mesh['grp'=2,'ep'=16,'tp'=1] {'ep'}, dimensions={0} | all-to-all | bytes 6291456 | tf_op jit(solution)/shard_map/all_to_all | solution.py:45
  191.7 1.9 multiply_reduce_fusion
  193.6 0.0 copy-done
  193.6 0.8 multiply_convert_fusion
  (4 shorter events, 0.1 us)
Async XLA Ops:
  3.6 81.7 %copy-start.1 = (bf16[1,2048,2048]{2,1,0:T(8,128)(2,1)S(1)}, bf16[1,2048,2048]{2,1,0:T(8,128)(2,1)}, u32[]{:S(2)}) copy-start(bf16[1,2048,2048]{2,1,0:T(8,128)(2,1)} %param.12) | copy-start | bytes 25165828
  116.7 76.9 %copy-start = (f32[2048]{0:T(1024)S(1)}, f32[2048]{0:T(1024)}, u32[]{:S(2)}) copy-start(f32[2048]{0:T(1024)} %param.15) | copy-start | bytes 24580
where the time goes:
time: 195 us; the launch traced here: 194 us
  blocking collectives  152 us (78%)
  matrix products  35.7 us (18%)
  other arithmetic  4.93 us (3%)
    all_to_all x1, blocking collectives, per_device(): lax.all_to_all(outgoing, 'ep', split_axis=0, concat_axis=0, tiled=True)  77.3 us
    all_to_all x1, blocking collectives, per_device(): lax.all_to_all(summed, 'ep', split_axis=0, concat_axis=0, tiled=True)  75 us
    dot_general x1, matrix products, per_device(): jnp.einsum('secf,efd->secd', hidden, w_down, preferred_element_type=jnp.f...  22.9 us
    dot_general x1, matrix products, per_device(): jnp.einsum('secd,edf->secf', received, w_gate, preferred_element_type=jnp...  8.55 us

commit v1 on v0

--- a/solution.py
+++ b/solution.py
@@ -5,6 +5,17 @@
 
 TOP_K = 6
 EPS = 1e-06
+
+
+def cut_along(x, dim, size):
+    before, after = (x.shape[:dim], x.shape[dim + 1 :])
+    return jnp.moveaxis(x.reshape(*before, size, -1, *after), dim, 0)
+
+
+def joined_along(blocks, dim):
+    lengths = list(blocks.shape[1:])
+    lengths[dim] *= blocks.shape[0]
+    return jnp.moveaxis(blocks, 0, dim).reshape(lengths)
 
 
 def slot_table(route_rows, experts_all, capacity):
@@ -42,7 +53,14 @@
     summed = lax.psum_scatter(
         partial_value.astype(jnp.bfloat16), "tp", scatter_dimension=3, tiled=True
     )
-    returned = lax.all_to_all(summed, "ep", split_axis=0, concat_axis=0, tiled=True)
+    size, place = (lax.axis_size("ep"), lax.axis_index("ep"))
+    tiles = cut_along(summed, 0, size)
+    outs = [tiles[place]]
+    for step in range(1, size):
+        sent = tiles[place ^ step]
+        outs.append(lax.ppermute(sent, "ep", [(i, i ^ step) for i in range(size)]))
+    tiles = jnp.stack(outs)[place ^ jnp.arange(size)]
+    returned = joined_along(tiles, 0)
     results = returned.reshape(slot_count, returned.shape[3]).astype(jnp.float32)
     combined = jnp.dot(combine_rows, results, precision=lax.Precision.HIGHEST)
     local_squares = jnp.sum(combined * combined, axis=1)

time: 195 us -> 211 us (1.082)
  the two profiles are of different devices: /device:TPU:1 before, /device:TPU:21 now
where the time goes in v1:
time: 211 us; the launch traced here: 210 us
  waiting for transfers between devices  117 us (55%)
  starting transfers between devices  40.6 us (19%)
  matrix products  39 us (18%)
  local copies, waits for them, and re-layouts  9 us (4%)
  other arithmetic  4.66 us (2%)
    all_to_all x1, waiting for transfers between devices, per_device(): lax.all_to_all(outgoing, 'ep', split_axis=0, concat_axis=0, tiled=True)  69.5 us
    ppermute x15, waiting for transfers between devices, per_device(): outs.append(lax.ppermute(sent, 'ep', [(i, i ^ step) for i in range(size)]))  47.3 us
    ppermute x15, starting transfers between devices, per_device(): outs.append(lax.ppermute(sent, 'ep', [(i, i ^ step) for i in range(size)]))  34.2 us
    dot_general x1, matrix products, per_device(): jnp.einsum('secf,efd->secd', hidden, w_down, preferred_element_type=jnp.f...  22.9 us
    dot_general x1, matrix products, per_device(): jnp.einsum('secd,edf->secf', received, w_gate, preferred_element_type=jnp...  10.7 us
    all_to_all x1, starting transfers between devices, per_device(): lax.all_to_all(outgoing, 'ep', split_axis=0, concat_axis=0, tiled=True)  6.43 us
  transfers between devices with their start and end apart: 16, of which 11 were waited for; matrix products, arithmetic and copies ran while one was open for 1% of the time, Pallas kernels for 0%

profile of v1, /device:TPU:21, one launch (start us, length us, event | category | flops | bytes accessed | tf_op | source)
XLA Modules:
  0.0 210.3 jit_solution(4417502161371064930)
XLA Ops:
  5.3 3.7 %convolution_convert_fusion = bf16[768,2048]{1,0:T(8,128)(2,1)} fusion(bf16[64,2048]{1,0:T(8,128)(2,1)} %param.8, f32[2048]{0:T(1024)} %param.9, f32[64]{0:T(128)S(1)} %add_rsqrt_fusion.1, bf16[64,768]{1,0:T(8,128)(2,1)S(1)} %get-tuple-element.5), kind=kOutput, calls=%fused_computation.15 | convolution fusion | flops 203423744 | bytes 3514624 | tf_op jit(solution)/shard_map/dot_general | solution.py:46
  9.0 6.4 %all-to-all-start = ((bf16[16,1,48,2048]{3,2,1,0:T(8,128)(2,1)}), bf16[16,1,48,2048]{3,2,1,0:T(8,128)(2,1)S(1)}, u32[]{:S(2)}, u32[]{:S(2)}) async-start(bf16[16,1,48,2048]{3,2,1,0:T(8,128)(2,1)} %bitcast.2), calls=%async_computation | async-start | bytes 6291456 | tf_op jit(solution)/shard_map/all_to_all | solution.py:48
  15.5 69.5 %all-to-all-done = bf16[16,1,48,2048]{3,2,1,0:T(8,128)(2,1)S(1)} async-done(((bf16[16,1,48,2048]{3,2,1,0:T(8,128)(2,1)}), bf16[16,1,48,2048]{3,2,1,0:T(8,128)(2,1)S(1)}, u32[]{:S(2)}, u32[]{:S(2)}) %all-to-all-start) | async-done | bytes 3145760 | tf_op jit(solution)/shard_map/all_to_all | solution.py:48
  84.9 10.7 %fusion.4 = f32[16,48,2048]{2,1,0:T(8,128)} fusion(bf16[1,2048,2048]{2,1,0:T(8,128)(2,1)} %param.12, bf16[16,1,48,2048]{3,2,1,0:T(8,128)(2,1)S(1)} %all-to-all-done), kind=kOutput, calls=%fused_computation.5 | convolution fusion | flops 6442450944 | bytes 17825792 | tf_op jit(solution)/shard_map/secd,edf->secf/dot_general | solution.py:49
  95.6 22.9 %fusion.12 = bf16[16,48,2048]{2,1,0:T(8,128)(2,1)} fusion(bf16[1,2048,2048]{2,1,0:T(8,128)(2,1)} %param.14, f32[16,48,2048]{2,1,0:T(8,128)} %fusion.4, bf16[1,2048,2048]{2,1,0:T(8,128)(2,1)} %param.13, bf16[16,1,48,2048]{3,2,1,0:T(8,128)(2,1)S(1)} %all-to-all-done), kind=kOutput, calls=%fused_computation.14 | convolution fusion | flops 12895911936 | bytes 29360128 | tf_op jit(solution)/shard_map/secf,efd->secd/dot_general | solution.py:52
  118.5 2.1 dynamic-slice_bitcast_fusion
  121.6 1.7 collective-permute-start.2
  123.3 1.8 collective-permute-start.4
  128.0 2.3 %collective-permute-start.6 = (bf16[1,1,48,2048]{3,2,1,0:T(8,128)(2,1)S(1)}, bf16[1,1,48,2048]{3,2,1,0:T(8,128)(2,1)S(1)}, u32[]{:S(2)}, u32[]{:S(2)}) collective-permute-start(bf16[1,1,48,2048]{3,2,1,0:T(8,128)(2,1)S(1)} %get-tuple-element.15), channel_id=1, source_target_pairs={{0,7},{1,6},{2,5},{3,4},{4,3},{5,2},{6,1},{7,0},{8,15},{9,14},{10,... | collective-permute-start | bytes 589832 | tf_op jit(solution)/shard_map/ppermute | solution.py:61
  130.3 2.4 %collective-permute-done.2 = bf16[1,1,48,2048]{3,2,1,0:T(8,128)(2,1)S(1)} collective-permute-done((bf16[1,1,48,2048]{3,2,1,0:T(8,128)(2,1)S(1)}, bf16[1,1,48,2048]{3,2,1,0:T(8,128)(2,1)S(1)}, u32[]{:S(2)}, u32[]{:S(2)}) %collective-permute-start.2) | collective-permute-done | bytes 196640 | tf_op jit(solution)/shard_map/ppermute | solution.py:61
  132.8 2.4 %collective-permute-start.8 = (bf16[1,1,48,2048]{3,2,1,0:T(8,128)(2,1)S(1)}, bf16[1,1,48,2048]{3,2,1,0:T(8,128)(2,1)S(1)}, u32[]{:S(2)}, u32[]{:S(2)}) collective-permute-start(bf16[1,1,48,2048]{3,2,1,0:T(8,128)(2,1)S(1)} %get-tuple-element.13), channel_id=1, source_target_pairs={{0,9},{1,8},{2,11},{3,10},{4,13},{5,12},{6,15},{7,14},{8,1},{9,0},... | collective-permute-start | bytes 589832 | tf_op jit(solution)/shard_map/ppermute | solution.py:61
  135.3 8.3 %collective-permute-done.5 = bf16[1,1,48,2048]{3,2,1,0:T(8,128)(2,1)S(1)} collective-permute-done((bf16[1,1,48,2048]{3,2,1,0:T(8,128)(2,1)S(1)}, bf16[1,1,48,2048]{3,2,1,0:T(8,128)(2,1)S(1)}, u32[]{:S(2)}, u32[]{:S(2)}) %collective-permute-start.5) | collective-permute-done | bytes 196640 | tf_op jit(solution)/shard_map/ppermute | solution.py:61
  143.7 4.7 %collective-permute-start.10 = (bf16[1,1,48,2048]{3,2,1,0:T(8,128)(2,1)S(1)}, bf16[1,1,48,2048]{3,2,1,0:T(8,128)(2,1)S(1)}, u32[]{:S(2)}, u32[]{:S(2)}) collective-permute-start(bf16[1,1,48,2048]{3,2,1,0:T(8,128)(2,1)S(1)} %get-tuple-element.11), channel_id=1, source_target_pairs={{0,11},{1,10},{2,9},{3,8},{4,15},{5,14},{6,13},{7,12},{8,3},{9,2},... | collective-permute-start | bytes 589832 | tf_op jit(solution)/shard_map/ppermute | solution.py:61
  149.1 1.3 collective-permute-start.12
  151.2 17.4 %collective-permute-start.13 = (bf16[1,1,48,2048]{3,2,1,0:T(8,128)(2,1)S(1)}, bf16[1,1,48,2048]{3,2,1,0:T(8,128)(2,1)S(1)}, u32[]{:S(2)}, u32[]{:S(2)}) collective-permute-start(bf16[1,1,48,2048]{3,2,1,0:T(8,128)(2,1)S(1)} %get-tuple-element.8), channel_id=1, source_target_pairs={{0,14},{1,15},{2,12},{3,13},{4,10},{5,11},{6,8},{7,9},{8,6},{9,7},... | collective-permute-start | bytes 589832 | tf_op jit(solution)/shard_map/ppermute | solution.py:61
  168.7 6.7 %collective-permute-done.9 = bf16[1,1,48,2048]{3,2,1,0:T(8,128)(2,1)S(1)} collective-permute-done((bf16[1,1,48,2048]{3,2,1,0:T(8,128)(2,1)S(1)}, bf16[1,1,48,2048]{3,2,1,0:T(8,128)(2,1)S(1)}, u32[]{:S(2)}, u32[]{:S(2)}) %collective-permute-start.9) | collective-permute-done | bytes 196640 | tf_op jit(solution)/shard_map/ppermute | solution.py:61
  175.4 4.2 %collective-permute-done.10 = bf16[1,1,48,2048]{3,2,1,0:T(8,128)(2,1)S(1)} collective-permute-done((bf16[1,1,48,2048]{3,2,1,0:T(8,128)(2,1)S(1)}, bf16[1,1,48,2048]{3,2,1,0:T(8,128)(2,1)S(1)}, u32[]{:S(2)}, u32[]{:S(2)}) %collective-permute-start.10) | collective-permute-done | bytes 196640 | tf_op jit(solution)/shard_map/ppermute | solution.py:61
  179.6 9.5 %collective-permute-done.11 = bf16[1,1,48,2048]{3,2,1,0:T(8,128)(2,1)S(1)} collective-permute-done((bf16[1,1,48,2048]{3,2,1,0:T(8,128)(2,1)S(1)}, bf16[1,1,48,2048]{3,2,1,0:T(8,128)(2,1)S(1)}, u32[]{:S(2)}, u32[]{:S(2)}) %collective-permute-start.11) | collective-permute-done | bytes 196640 | tf_op jit(solution)/shard_map/ppermute | solution.py:61
  189.2 4.5 %collective-permute-done.12 = bf16[1,1,48,2048]{3,2,1,0:T(8,128)(2,1)S(1)} collective-permute-done((bf16[1,1,48,2048]{3,2,1,0:T(8,128)(2,1)S(1)}, bf16[1,1,48,2048]{3,2,1,0:T(8,128)(2,1)S(1)}, u32[]{:S(2)}, u32[]{:S(2)}) %collective-permute-start.12) | collective-permute-done | bytes 196640 | tf_op jit(solution)/shard_map/ppermute | solution.py:61
  193.7 5.4 %collective-permute-done.13 = bf16[1,1,48,2048]{3,2,1,0:T(8,128)(2,1)S(1)} collective-permute-done((bf16[1,1,48,2048]{3,2,1,0:T(8,128)(2,1)S(1)}, bf16[1,1,48,2048]{3,2,1,0:T(8,128)(2,1)S(1)}, u32[]{:S(2)}, u32[]{:S(2)}) %collective-permute-start.13) | collective-permute-done | bytes 196640 | tf_op jit(solution)/shard_map/ppermute | solution.py:61
  199.1 4.2 %collective-permute-done.14 = bf16[1,1,48,2048]{3,2,0,1:T(8,128)(2,1)S(1)} collective-permute-done((bf16[1,1,48,2048]{3,2,0,1:T(8,128)(2,1)S(1)}, bf16[1,1,48,2048]{3,2,0,1:T(8,128)(2,1)S(1)}, u32[]{:S(2)}, u32[]{:S(2)}) %collective-permute-start.14) | collective-permute-done | bytes 196640 | tf_op jit(solution)/shard_map/ppermute | solution.py:61
  203.3 1.7 copy-done
  205.0 2.6 %gather_fusion = bf16[16,48,2048]{2,1,0:T(8,128)(2,1)S(1)} fusion(bf16[16,48,2048]{2,1,0:T(8,128)(2,1)} %bitcast.221, s32[1024]{0:T(1024)S(1)} %pad_clamp_fusion), kind=kCustom, calls=%fused_computation | custom fusion | bytes 6291520 | tf_op jit(solution)/shard_map/gather | solution.py:62
  207.6 1.9 multiply_reduce_fusion
  (52 shorter events, 11.9 us)
Async XLA Ops:
  9.0 75.9 %all-to-all-start = ((bf16[16,1,48,2048]{3,2,1,0:T(8,128)(2,1)}), bf16[16,1,48,2048]{3,2,1,0:T(8,128)(2,1)S(1)}, u32[]{:S(2)}, u32[]{:S(2)}) async-start(bf16[16,1,48,2048]{3,2,1,0:T(8,128)(2,1)} %bitcast.2), calls=%async_computation | async-start | bytes 6291456 | tf_op jit(solution)/shard_map/all_to_all | solution.py:48
  120.6 5.5 %collective-permute-start = (bf16[1,1,48,2048]{3,2,1,0:T(8,128)(2,1)S(1)}, bf16[1,1,48,2048]{3,2,1,0:T(8,128)(2,1)S(1)}, u32[]{:S(2)}, u32[]{:S(2)}) collective-permute-start(bf16[1,1,48,2048]{3,2,1,0:T(8,128)(2,1)S(1)} %get-tuple-element.21), channel_id=1, source_target_pairs={{0,1},{1,0},{2,3},{3,2},{4,5},{5,4},{6,7},{7,6},{8,9},{9,8},{10,11... | collective-permute-start | bytes 589832 | tf_op jit(solution)/shard_map/ppermute | solution.py:61
  121.6 6.4 %collective-permute-start.1 = (bf16[1,1,48,2048]{3,2,1,0:T(8,128)(2,1)S(1)}, bf16[1,1,48,2048]{3,2,1,0:T(8,128)(2,1)S(1)}, u32[]{:S(2)}, u32[]{:S(2)}) collective-permute-start(bf16[1,1,48,2048]{3,2,1,0:T(8,128)(2,1)S(1)} %get-tuple-element.20), channel_id=1, source_target_pairs={{0,2},{1,3},{2,0},{3,1},{4,6},{5,7},{6,4},{7,5},{8,10},{9,11},{10,... | collective-permute-start | bytes 589832 | tf_op jit(solution)/shard_map/ppermute | solution.py:61
  121.6 11.1 %collective-permute-start.2 = (bf16[1,1,48,2048]{3,2,1,0:T(8,128)(2,1)S(1)}, bf16[1,1,48,2048]{3,2,1,0:T(8,128)(2,1)S(1)}, u32[]{:S(2)}, u32[]{:S(2)}) collective-permute-start(bf16[1,1,48,2048]{3,2,1,0:T(8,128)(2,1)S(1)} %get-tuple-element.19), channel_id=1, source_target_pairs={{0,3},{1,2},{2,1},{3,0},{4,7},{5,6},{6,5},{7,4},{8,11},{9,10},{10,... | collective-permute-start | bytes 589832 | tf_op jit(solution)/shard_map/ppermute | solution.py:61
  123.3 9.4 %collective-permute-start.3 = (bf16[1,1,48,2048]{3,2,1,0:T(8,128)(2,1)S(1)}, bf16[1,1,48,2048]{3,2,1,0:T(8,128)(2,1)S(1)}, u32[]{:S(2)}, u32[]{:S(2)}) collective-permute-start(bf16[1,1,48,2048]{3,2,1,0:T(8,128)(2,1)S(1)} %get-tuple-element.18), channel_id=1, source_target_pairs={{0,4},{1,5},{2,6},{3,7},{4,0},{5,1},{6,2},{7,3},{8,12},{9,13},{10,... | collective-permute-start | bytes 589832 | tf_op jit(solution)/shard_map/ppermute | solution.py:61
  123.3 11.9 %collective-permute-start.4 = (bf16[1,1,48,2048]{3,2,1,0:T(8,128)(2,1)S(1)}, bf16[1,1,48,2048]{3,2,1,0:T(8,128)(2,1)S(1)}, u32[]{:S(2)}, u32[]{:S(2)}) collective-permute-start(bf16[1,1,48,2048]{3,2,1,0:T(8,128)(2,1)S(1)} %get-tuple-element.17), channel_id=1, source_target_pairs={{0,5},{1,4},{2,7},{3,6},{4,1},{5,0},{6,3},{7,2},{8,13},{9,12},{10,... | collective-permute-start | bytes 589832 | tf_op jit(solution)/shard_map/ppermute | solution.py:61
  126.0 17.6 %collective-permute-start.5 = (bf16[1,1,48,2048]{3,2,1,0:T(8,128)(2,1)S(1)}, bf16[1,1,48,2048]{3,2,1,0:T(8,128)(2,1)S(1)}, u32[]{:S(2)}, u32[]{:S(2)}) collective-permute-start(bf16[1,1,48,2048]{3,2,1,0:T(8,128)(2,1)S(1)} %get-tuple-element.16), channel_id=1, source_target_pairs={{0,6},{1,7},{2,4},{3,5},{4,2},{5,3},{6,0},{7,1},{8,14},{9,15},{10,... | collective-permute-start | bytes 589832 | tf_op jit(solution)/shard_map/ppermute | solution.py:61
  128.0 20.4 %collective-permute-start.6 = (bf16[1,1,48,2048]{3,2,1,0:T(8,128)(2,1)S(1)}, bf16[1,1,48,2048]{3,2,1,0:T(8,128)(2,1)S(1)}, u32[]{:S(2)}, u32[]{:S(2)}) collective-permute-start(bf16[1,1,48,2048]{3,2,1,0:T(8,128)(2,1)S(1)} %get-tuple-element.15), channel_id=1, source_target_pairs={{0,7},{1,6},{2,5},{3,4},{4,3},{5,2},{6,1},{7,0},{8,15},{9,14},{10,... | collective-permute-start | bytes 589832 | tf_op jit(solution)/shard_map/ppermute | solution.py:61
  132.7 16.3 %collective-permute-start.7 = (bf16[1,1,48,2048]{3,2,1,0:T(8,128)(2,1)S(1)}, bf16[1,1,48,2048]{3,2,1,0:T(8,128)(2,1)S(1)}, u32[]{:S(2)}, u32[]{:S(2)}) collective-permute-start(bf16[1,1,48,2048]{3,2,1,0:T(8,128)(2,1)S(1)} %get-tuple-element.14), channel_id=1, source_target_pairs={{0,8},{1,9},{2,10},{3,11},{4,12},{5,13},{6,14},{7,15},{8,0},{9,1},... | collective-permute-start | bytes 589832 | tf_op jit(solution)/shard_map/ppermute | solution.py:61
  132.8 18.5 %collective-permute-start.8 = (bf16[1,1,48,2048]{3,2,1,0:T(8,128)(2,1)S(1)}, bf16[1,1,48,2048]{3,2,1,0:T(8,128)(2,1)S(1)}, u32[]{:S(2)}, u32[]{:S(2)}) collective-permute-start(bf16[1,1,48,2048]{3,2,1,0:T(8,128)(2,1)S(1)} %get-tuple-element.13), channel_id=1, source_target_pairs={{0,9},{1,8},{2,11},{3,10},{4,13},{5,12},{6,15},{7,14},{8,1},{9,0},... | collective-permute-start | bytes 589832 | tf_op jit(solution)/shard_map/ppermute | solution.py:61
  135.2 40.2 %collective-permute-start.9 = (bf16[1,1,48,2048]{3,2,1,0:T(8,128)(2,1)S(1)}, bf16[1,1,48,2048]{3,2,1,0:T(8,128)(2,1)S(1)}, u32[]{:S(2)}, u32[]{:S(2)}) collective-permute-start(bf16[1,1,48,2048]{3,2,1,0:T(8,128)(2,1)S(1)} %get-tuple-element.12), channel_id=1, source_target_pairs={{0,10},{1,11},{2,8},{3,9},{4,14},{5,15},{6,12},{7,13},{8,2},{9,3},... | collective-permute-start | bytes 589832 | tf_op jit(solution)/shard_map/ppermute | solution.py:61
  143.7 35.9 %collective-permute-start.10 = (bf16[1,1,48,2048]{3,2,1,0:T(8,128)(2,1)S(1)}, bf16[1,1,48,2048]{3,2,1,0:T(8,128)(2,1)S(1)}, u32[]{:S(2)}, u32[]{:S(2)}) collective-permute-start(bf16[1,1,48,2048]{3,2,1,0:T(8,128)(2,1)S(1)} %get-tuple-element.11), channel_id=1, source_target_pairs={{0,11},{1,10},{2,9},{3,8},{4,15},{5,14},{6,13},{7,12},{8,3},{9,2},... | collective-permute-start | bytes 589832 | tf_op jit(solution)/shard_map/ppermute | solution.py:61
  148.4 40.8 %collective-permute-start.11 = (bf16[1,1,48,2048]{3,2,1,0:T(8,128)(2,1)S(1)}, bf16[1,1,48,2048]{3,2,1,0:T(8,128)(2,1)S(1)}, u32[]{:S(2)}, u32[]{:S(2)}) collective-permute-start(bf16[1,1,48,2048]{3,2,1,0:T(8,128)(2,1)S(1)} %get-tuple-element.10), channel_id=1, source_target_pairs={{0,12},{1,13},{2,14},{3,15},{4,8},{5,9},{6,10},{7,11},{8,4},{9,5},... | collective-permute-start | bytes 589832 | tf_op jit(solution)/shard_map/ppermute | solution.py:61
  149.1 44.6 %collective-permute-start.12 = (bf16[1,1,48,2048]{3,2,1,0:T(8,128)(2,1)S(1)}, bf16[1,1,48,2048]{3,2,1,0:T(8,128)(2,1)S(1)}, u32[]{:S(2)}, u32[]{:S(2)}) collective-permute-start(bf16[1,1,48,2048]{3,2,1,0:T(8,128)(2,1)S(1)} %get-tuple-element.9), channel_id=1, source_target_pairs={{0,13},{1,12},{2,15},{3,14},{4,9},{5,8},{6,11},{7,10},{8,5},{9,4},... | collective-permute-start | bytes 589832 | tf_op jit(solution)/shard_map/ppermute | solution.py:61
  151.2 47.8 %collective-permute-start.13 = (bf16[1,1,48,2048]{3,2,1,0:T(8,128)(2,1)S(1)}, bf16[1,1,48,2048]{3,2,1,0:T(8,128)(2,1)S(1)}, u32[]{:S(2)}, u32[]{:S(2)}) collective-permute-start(bf16[1,1,48,2048]{3,2,1,0:T(8,128)(2,1)S(1)} %get-tuple-element.8), channel_id=1, source_target_pairs={{0,14},{1,15},{2,12},{3,13},{4,10},{5,11},{6,8},{7,9},{8,6},{9,7},... | collective-permute-start | bytes 589832 | tf_op jit(solution)/shard_map/ppermute | solution.py:61
  175.4 27.9 %collective-permute-start.14 = (bf16[1,1,48,2048]{3,2,0,1:T(8,128)(2,1)S(1)}, bf16[1,1,48,2048]{3,2,0,1:T(8,128)(2,1)S(1)}, u32[]{:S(2)}, u32[]{:S(2)}) collective-permute-start(bf16[1,1,48,2048]{3,2,0,1:T(8,128)(2,1)S(1)} %get-tuple-element.7), channel_id=1, source_target_pairs={{0,15},{1,14},{2,13},{3,12},{4,11},{5,10},{6,9},{7,8},{8,7},{9,6},... | collective-permute-start | bytes 589832 | tf_op jit(solution)/shard_map/ppermute | solution.py:61
  203.3 1.7 copy-start
  207.6 1.9 copy-start.1
